TPU v7x, 128 devices: a whole 4x4x4 slice. The times are simulated.
128 devices in a mesh: fs: 16 (over z, x), tp: 8 (over y, core).
Axes of the slice: x: 4, y: 4, z: 4, core: 2. Of those that a mesh axis runs over, the one named last changes fastest.
Arguments:
- mixer_input: bfloat16 [16384, 4096], P('fs'), may hold values from -6 to 6
- cell_output: bfloat16 [16384, 2048], P('fs'), may hold values from -6 to 6
- query_grad: bfloat16 [16384, 2048], P('fs', 'tp'), may hold values from -4 to 4
- value_grad: bfloat16 [16384, 2048], P('fs', 'tp'), may hold values from -4 to 4
- output_grad: bfloat16 [16384, 4096], P('fs', 'tp'), may hold values from -4 to 4
- query_weight: float32 [4096, 2048], P('fs', 'tp'), may hold values from -6 to 6
- value_weight: float32 [4096, 2048], P('fs', 'tp'), may hold values from -6 to 6
- output_weight: float32 [2048, 4096], P('fs', 'tp'), may hold values from -6 to 6
- query_basis: bfloat16 [4096, 128], P('fs'), may hold values from -0.09375 to 0.09375
- value_basis: bfloat16 [4096, 128], P('fs'), may hold values from -0.09375 to 0.09375
- output_basis: bfloat16 [2048, 128], P('fs'), may hold values from -0.125 to 0.125
- query_mean: float32 [128, 2048], P(None, 'tp'), may hold values from -6 to 6
- value_mean: float32 [128, 2048], P(None, 'tp'), may hold values from -6 to 6
- output_mean: float32 [128, 4096], P(None, 'tp'), may hold values from -6 to 6
- query_square: float32 [128, 2048], P(None, 'tp'), may hold values from 0.25 to 4
- value_square: float32 [128, 2048], P(None, 'tp'), may hold values from 0.25 to 4
- output_square: float32 [128, 4096], P(None, 'tp'), may hold values from 0.25 to 4
Outputs:
- query_step: float32 [4096, 2048], P('fs', 'tp')
- value_step: float32 [4096, 2048], P('fs', 'tp')
- output_step: float32 [2048, 4096], P('fs', 'tp')
- query_copy: bfloat16 [4096, 2048], P(None, 'tp')
- value_copy: bfloat16 [4096, 2048], P(None, 'tp')
- output_copy: bfloat16 [2048, 4096], P(None, 'tp')
- query_first: float32 [128, 2048], P(None, 'tp')
- value_first: float32 [128, 2048], P(None, 'tp')
- output_first: float32 [128, 4096], P(None, 'tp')
- query_second: float32 [128, 2048], P(None, 'tp')
- value_second: float32 [128, 2048], P(None, 'tp')
- output_second: float32 [128, 4096], P(None, 'tp')
All inputs are finite; a program needn't handle non-finite values.
Results may differ from a plain program's by a relative error of at most 0.013.
Values may be sent and summed in bfloat16 or wider, within the bound.
A program may use at most 128 MiB of HBM per device.

v0:
```python
import jax
import jax.numpy as jnp
from jax import lax
from jax.sharding import PartitionSpec as P

MODEL = 4096
CELL = 2048


beta_first = 0.8
beta_second = 0.9
floor_mean = 0.005
learn_rate = 0.05


def side_by_side(arrays, axis, dim, along):
    ends, at = ([], 0)
    for a in arrays[:-1]:
        at += a.shape[along]
        ends.append(at)
    both = jnp.concatenate(arrays, axis=along)
    return tuple(jnp.split(lax.all_gather(both, axis, axis=dim, tiled=True), ends, axis=along))


def in_order(pieces, dim):
    dims = list(pieces.shape[1:])
    dims[dim] *= pieces.shape[0]
    return jnp.moveaxis(pieces, 0, dim).reshape(dims)


def sent_to_all(x, axis):
    peers = lax.axis_size(axis)
    return lax.all_to_all(jnp.broadcast_to(x[None], (peers, *x.shape)), axis, 0, 0, tiled=True)


def gathered_copies(x, axis, dim):
    return in_order(sent_to_all(x, axis), dim)


def taken_together(x, axis):
    return sent_to_all(x, axis).sum(axis=0)


def one_gather(arrays, axis, dims):
    ravelled = jnp.concatenate([a.reshape(-1) for a in arrays])
    lines, at, outs = (lax.all_gather(ravelled, axis), 0, [])
    for a, dim in zip(arrays, dims):
        pieces = lines[:, at : at + a.size].reshape(-1, *a.shape)
        outs.append(in_order(pieces, dim))
        at += a.size
    return tuple(outs)


def across(leading, trailing):
    return lax.dot_general(
        leading, trailing, (((0,), (0,)), ((), ())), preferred_element_type=jnp.float32
    )


def across_exact(leading, trailing):
    return lax.dot_general(
        leading,
        trailing,
        (((0,), (0,)), ((), ())),
        precision=lax.Precision.HIGHEST,
        preferred_element_type=jnp.float32,
    )


def product_exact(leading, trailing):
    return jnp.dot(
        leading, trailing, precision=lax.Precision.HIGHEST, preferred_element_type=jnp.float32
    )


def moments(projected, mean_old, square_old):
    moment_one = beta_first * mean_old + (1.0 - beta_first) * projected
    moment_two = beta_second * square_old + (1.0 - beta_second) * projected * projected
    return (moment_one, moment_two, moment_one / jnp.sqrt(moment_two))


def local(
    mixer_input,
    cell_output,
    query_grad,
    value_grad,
    output_grad,
    query_weight,
    value_weight,
    output_weight,
    query_basis,
    value_basis,
    output_basis,
    query_mean,
    value_mean,
    output_mean,
    query_square,
    value_square,
    output_square,
):
    local_query = query_basis.astype(jnp.float32)
    local_value = value_basis.astype(jnp.float32)
    local_output = output_basis.astype(jnp.float32)
    pieces = side_by_side((query_basis, value_basis), "fs", 0, 1)
    window = mixer_input
    first_sum = across_exact(pieces[0].astype(jnp.float32), across(window, query_grad))
    second_sum = across_exact(pieces[1].astype(jnp.float32), across(window, value_grad))
    window = cell_output
    part_output = across_exact(
        gathered_copies(output_basis, "fs", 0).astype(jnp.float32), across(window, output_grad)
    )
    gram_query = across_exact(local_query, local_query)
    gram_value = across_exact(local_value, local_value)
    gram_output = across_exact(local_output, local_output)
    proj_query, proj_value, proj_output, gram_query, gram_value, gram_output = lax.psum(
        (first_sum, second_sum, part_output, gram_query, gram_value, gram_output), "fs"
    )
    query_first, query_second, query_dir = moments(proj_query, query_mean, query_square)
    value_first, value_second, value_dir = moments(proj_value, value_mean, value_square)
    output_first, output_second, output_dir = moments(proj_output, output_mean, output_square)
    low_query = product_exact(local_query, query_dir)
    low_value = product_exact(local_value, value_dir)
    low_output = product_exact(local_output, output_dir)
    partial_squares = jnp.sum(gram_query * product_exact(query_dir, query_dir.T))
    partial_squares = partial_squares + jnp.sum(gram_value * product_exact(value_dir, value_dir.T))
    partial_squares = partial_squares + jnp.sum(
        gram_output * product_exact(output_dir, output_dir.T)
    )
    squares = taken_together(partial_squares, "tp")
    factor = 1.0 / jnp.sqrt(squares / (3.0 * MODEL * CELL) + floor_mean)
    query_step = -factor * low_query
    value_step = -factor * low_value
    output_step = -factor * low_output
    query_copy, value_copy, output_copy = one_gather(
        (
            (query_weight + learn_rate * query_step).astype(jnp.bfloat16),
            (value_weight + learn_rate * value_step).astype(jnp.bfloat16),
            (output_weight + learn_rate * output_step).astype(jnp.bfloat16),
        ),
        "fs",
        (0, 0, 0),
    )
    return (
        query_step,
        value_step,
        output_step,
        query_copy,
        value_copy,
        output_copy,
        query_first,
        value_first,
        output_first,
        query_second,
        value_second,
        output_second,
    )


def solution(mesh):
    in_specs = (
        P("fs", None),
        P("fs", None),
        P("fs", "tp"),
        P("fs", "tp"),
        P("fs", "tp"),
        P("fs", "tp"),
        P("fs", "tp"),
        P("fs", "tp"),
        P("fs", None),
        P("fs", None),
        P("fs", None),
        P(None, "tp"),
        P(None, "tp"),
        P(None, "tp"),
        P(None, "tp"),
        P(None, "tp"),
        P(None, "tp"),
    )
    out_specs = (
        P("fs", "tp"),
        P("fs", "tp"),
        P("fs", "tp"),
        P(None, "tp"),
        P(None, "tp"),
        P(None, "tp"),
        P(None, "tp"),
        P(None, "tp"),
        P(None, "tp"),
        P(None, "tp"),
        P(None, "tp"),
        P(None, "tp"),
    )
    return jax.shard_map(local, mesh=mesh, in_specs=in_specs, out_specs=out_specs, check_vma=False)
```

profile of v0, /device:TPU:0, one launch (start us, length us, event | category | flops | bytes accessed | tf_op | source)
XLA Modules:
  0.0 266.3 jit_solution(10231013794238130630)
XLA Ops:
  8.9 1.7 broadcast_in_dim.4
  10.5 8.0 %all-to-all-start = ((bf16[16,128,128]{2,1,0:T(8,128)(2,1)}), bf16[16,128,128]{2,1,0:T(8,128)(2,1)S(1)}, u32[]{:S(2)}, u32[]{:S(2)}) async-start(bf16[16,128,128]{2,1,0:T(8,128)(2,1)} %broadcast_in_dim.4), calls=%async_computation | async-start | bytes 1048576 | tf_op jit(solution)/shard_map/all_to_all | solution.py:33
  18.6 1.6 fusion.18
  20.2 1.8 fusion.14
  22.1 1.7 fusion.16
  23.8 8.0 %fusion.15 = f32[4096,256]{1,0:T(8,128)} fusion(bf16[1024,4096]{1,0:T(8,128)(2,1)} %param.17, bf16[1024,256]{1,0:T(8,128)(2,1)} %param.19), kind=kOutput, calls=%fused_computation.36 | convolution fusion | flops 2147483648 | bytes 13107200 | tf_op jit(solution)/shard_map/dot_general | solution.py:55
  31.8 4.6 %fusion.17 = f32[4096,256]{1,0:T(8,128)} fusion(bf16[1024,4096]{1,0:T(8,128)(2,1)S(1)} %bitcast.42, bf16[1024,256]{1,0:T(8,128)(2,1)S(1)} %copy-done.14), kind=kOutput, calls=%fused_computation.38 | convolution fusion | flops 2147483648 | bytes 13107200 | tf_op jit(solution)/shard_map/dot_general | solution.py:55
  36.5 4.4 %fusion.19 = f32[2048,512]{1,0:T(8,128)} fusion(bf16[1024,2048]{1,0:T(8,128)(2,1)S(1)} %copy-done.13, bf16[1024,512]{1,0:T(8,128)(2,1)S(1)} %copy-done), kind=kOutput, calls=%fused_computation.40 | convolution fusion | flops 2147483648 | bytes 9437184 | tf_op jit(solution)/shard_map/dot_general | solution.py:55
  40.9 6.3 %convolution_bitcast_fusion = f32[128,512]{0,1:T(8,128)} fusion(f32[2048,512]{1,0:T(8,128)} %fusion.19, bf16[2048,128]{1,0:T(8,128)(2,1)S(1)} %bitcast.34), kind=kOutput, calls=%fused_computation.6 | convolution fusion | flops 1610612736 | bytes 4980736 | tf_op jit(solution)/shard_map/dot_general | solution.py:61
  47.2 11.7 %all-gather.4.cloned.1.call-done = bf16[4096,256]{1,0:T(8,128)(2,1)} async-done(((bf16[256,256]{1,0:T(8,128)(2,1)}), bf16[4096,256]{1,0:T(8,128)(2,1)}) %all-gather.4.cloned.1.call-update) | async-done | bytes 2097168 | tf_op jit(solution)/shard_map/all_gather | solution.py:22
  59.0 5.4 %fusion.5 = f32[128,256]{1,0:T(8,128)} fusion(f32[4096,256]{1,0:T(8,128)} %fusion.15, bf16[4096,256]{1,0:T(8,128)(2,1)} %all-gather.4.cloned.1.call-done), kind=kOutput, calls=%fused_computation.12 | convolution fusion | flops 1610612736 | bytes 5373952 | tf_op jit(solution)/shard_map/dot_general | solution.py:61
  64.4 3.9 %fusion.3 = f32[128,256]{1,0:T(8,128)} fusion(f32[4096,256]{1,0:T(8,128)S(1)} %copy-done.1, bf16[4096,256]{1,0:T(8,128)(2,1)} %all-gather.4.cloned.1.call-done), kind=kOutput, calls=%fused_computation.10 | convolution fusion | flops 1610612736 | bytes 5373952 | tf_op jit(solution)/shard_map/dot_general | solution.py:61
  69.0 85.9 %all-reduce.3.cloned.1.call-done = (f32[128,128]{1,0:T(8,128)}, f32[128,256]{1,0:T(8,128)}, f32[128,128]{1,0:T(8,128)}, f32[128,256]{1,0:T(8,128)}, f32[128,128]{1,0:T(8,128)}, /*index=5*/f32[128,512]{0,1:T(8,128)}) async-done(((f32[128,128]{1,0:T(8,128)}, f32[128,256]{1,0:T(8,128)}, f32[128,128]{1,0:T(8,128)}, f32[128,256]{1,0:T(8,128)}, f32[128,128]{1,0:T(8,128)}, /*index=5*/f32[128,512]{0,1:T(8,128)}), ...) | async-done | bytes 720912 | tf_op jit(solution)/shard_map/psum | solution.py:115
  156.2 1.8 fusion.9
  158.0 1.7 fusion.8
  162.1 2.0 fusion.7
  164.8 9.4 %all_to_all.11 = f32[8,1,1]{2,1,0:T(1,128)S(1)} all-to-all(f32[8,1,1]{2,1,0:T(1,128)S(1)} %broadcast_in_dim.5), channel_id=1, replica_groups=mesh['fs'=16,'tp'=8] {'tp'}, dimensions={0} | all-to-all | bytes 64 | tf_op jit(solution)/shard_map/all_to_all | solution.py:33
  179.1 1.7 pad_maximum_fusion
  185.1 54.9 %all-gather.6.cloned.1.call-done = bf16[3145728]{0:T(1024)(128)(2,1)} async-done(((bf16[196608]{0:T(1024)(128)(2,1)}), bf16[3145728]{0:T(1024)(128)(2,1)}) %all-gather.6.cloned.1.call-update) | async-done | bytes 6291472 | tf_op jit(solution)/shard_map/all_gather | solution.py:46
  240.0 6.2 %reshape.44 = bf16[16,196608]{1,0:T(8,128)(2,1)} reshape(bf16[3145728]{0:T(1024)(128)(2,1)} %all-gather.6.cloned.1.call-done) | data formatting | bytes 12582912 | tf_op jit(solution)/shard_map/all_gather | solution.py:46
  246.2 5.3 %fusion.13 = (bf16[16,65536]{1,0:T(8,128)(2,1)}, bf16[16,65536]{1,0:T(8,128)(2,1)}, bf16[16,65536]{1,0:T(8,128)(2,1)S(1)}) fusion(bf16[16,196608]{1,0:T(8,128)(2,1)} %reshape.44), kind=kLoop, calls=%fused_computation.34 | loop fusion | bytes 12582912 | tf_op jit(solution)/shard_map/slice | solution.py:48
  251.5 3.2 %reshape_reshape.11 = bf16[2048,512]{1,0:T(8,128)(2,1)} reshape(bf16[16,65536]{1,0:T(8,128)(2,1)} %get-tuple-element.78) | data formatting | bytes 4194304 | tf_op jit(solution)/shard_map/reshape;reshape | solution.py:28
  254.7 3.2 %reshape_reshape.10 = bf16[4096,256]{1,0:T(8,128)(2,1)} reshape(bf16[16,65536]{1,0:T(8,128)(2,1)} %get-tuple-element.79) | data formatting | bytes 4194304 | tf_op jit(solution)/shard_map/reshape;reshape | solution.py:28
  257.8 1.9 reshape_reshape.9
  (66 shorter events, 13.2 us)
Async XLA Ops:
  7.2 29.3 %copy-start = (bf16[1024,512]{1,0:T(8,128)(2,1)S(1)}, bf16[1024,512]{1,0:T(8,128)(2,1)}, u32[]{:S(2)}) copy-start(bf16[1024,512]{1,0:T(8,128)(2,1)} %param.21) | copy-start | bytes 3145732
  7.2 51.8 %all-gather.4.cloned.1.call-start = ((), (), s32[]{:S(2)}) async-start(), calls=%async_computation.2 | async-start | bytes 2228224 | tf_op jit(solution)/shard_map/all_gather | solution.py:22
  10.5 30.4 %all-to-all-start = ((bf16[16,128,128]{2,1,0:T(8,128)(2,1)}), bf16[16,128,128]{2,1,0:T(8,128)(2,1)S(1)}, u32[]{:S(2)}, u32[]{:S(2)}) async-start(bf16[16,128,128]{2,1,0:T(8,128)(2,1)} %broadcast_in_dim.4), calls=%async_computation | async-start | bytes 1048576 | tf_op jit(solution)/shard_map/all_to_all | solution.py:33
  18.5 136.4 %all-reduce.3.cloned.1.call-start = ((), (), s32[]{:S(2)}) async-start(), calls=%async_computation.4 | async-start | bytes 1441792 | tf_op jit(solution)/shard_map/psum | solution.py:115
  20.2 11.6 %slice-start = ((s8[8388608]{0:T(1024)(128)(4,1)}), s8[4194304]{0:T(1024)(128)(4,1)S(1)}, s32[]{:S(2)}) async-start(s8[8388608]{0:T(1024)(128)(4,1)} %bitcast.41), calls=%async_computation.5 | async-start | bytes 8388608
  23.8 8.0 %slice-start.1 = ((s8[8388608]{0:T(1024)(128)(4,1)}), s8[4194304]{0:T(1024)(128)(4,1)S(1)}, s32[]{:S(2)}) async-start(s8[8388608]{0:T(1024)(128)(4,1)} %bitcast.41), calls=%async_computation.6 | async-start | bytes 8388608
  23.8 8.0 %copy-start.14 = (bf16[1024,256]{1,0:T(8,128)(2,1)S(1)}, bf16[1024,256]{1,0:T(8,128)(2,1)}, u32[]{:S(2)}) copy-start(bf16[1024,256]{1,0:T(8,128)(2,1)} %param.20) | copy-start | bytes 1572868
  31.8 4.6 %copy-start.13 = (bf16[1024,2048]{1,0:T(8,128)(2,1)S(1)}, bf16[1024,2048]{1,0:T(8,128)(2,1)}, u32[]{:S(2)}) copy-start(bf16[1024,2048]{1,0:T(8,128)(2,1)} %param.18) | copy-start | bytes 12582916
  59.0 5.4 %copy-start.1 = (f32[4096,256]{1,0:T(8,128)S(1)}, f32[4096,256]{1,0:T(8,128)}, u32[]{:S(2)}) copy-start(f32[4096,256]{1,0:T(8,128)} %fusion.17) | copy-start | bytes 12582916
  64.3 4.0 %copy-start.8 = (f32[256,256]{1,0:T(8,128)S(1)}, f32[256,256]{1,0:T(8,128)}, u32[]{:S(2)}) copy-start(f32[256,256]{1,0:T(8,128)} %param.22) | copy-start | bytes 786436
  64.3 4.1 %copy-start.9 = (f32[256,256]{1,0:T(8,128)S(1)}, f32[256,256]{1,0:T(8,128)}, u32[]{:S(2)}) copy-start(f32[256,256]{1,0:T(8,128)} %param.23) | copy-start | bytes 786436
  64.3 4.3 %copy-start.10 = (f32[128,512]{1,0:T(8,128)S(1)}, f32[128,512]{1,0:T(8,128)}, u32[]{:S(2)}) copy-start(f32[128,512]{1,0:T(8,128)} %param.24) | copy-start | bytes 786436
  64.3 4.4 %copy-start.11 = (f32[128,512]{1,0:T(8,128)S(1)}, f32[128,512]{1,0:T(8,128)}, u32[]{:S(2)}) copy-start(f32[128,512]{1,0:T(8,128)} %param.30) | copy-start | bytes 786436
  64.4 4.6 %copy-start.12 = (f32[128,512]{1,0:T(8,128)S(1)}, f32[128,512]{1,0:T(8,128)}, u32[]{:S(2)}) copy-start(f32[128,512]{1,0:T(8,128)} %param.33) | copy-start | bytes 786436
  68.3 109.1 %copy-start.6 = (bf16[256,128]{1,0:T(8,128)(2,1)S(1)}, bf16[256,128]{1,0:T(8,128)(2,1)}, u32[]{:S(2)}) copy-start(bf16[256,128]{1,0:T(8,128)(2,1)} %param.26) | copy-start | bytes 196612
  68.3 171.8 %all-gather.6.cloned.1.call-start = ((), (), s32[]{:S(2)}) async-start(), calls=%async_computation.3 | async-start | bytes 6684672 | tf_op jit(solution)/shard_map/all_gather | solution.py:46
  68.8 109.8 %copy-start.7 = (bf16[256,128]{1,0:T(8,128)(2,1)S(1)}, bf16[256,128]{1,0:T(8,128)(2,1)}, u32[]{:S(2)}) copy-start(bf16[256,128]{1,0:T(8,128)(2,1)} %param.25) | copy-start | bytes 196612
  156.2 24.7 %copy-start.2 = (f32[128,256]{1,0:T(8,128)}, f32[128,256]{1,0:T(8,128)S(1)}, u32[]{:S(2)}) copy-start(f32[128,256]{1,0:T(8,128)S(1)} %get-tuple-element.85) | copy-start | bytes 393220
  156.2 24.7 %copy-start.3 = (f32[128,256]{1,0:T(8,128)}, f32[128,256]{1,0:T(8,128)S(1)}, u32[]{:S(2)}) copy-start(f32[128,256]{1,0:T(8,128)S(1)} %get-tuple-element.86) | copy-start | bytes 393220
  156.2 24.7 %copy-start.4 = (f32[128,256]{1,0:T(8,128)}, f32[128,256]{1,0:T(8,128)S(1)}, u32[]{:S(2)}) copy-start(f32[128,256]{1,0:T(8,128)S(1)} %get-tuple-element.93) | copy-start | bytes 393220
  156.2 24.7 %copy-start.5 = (f32[128,256]{1,0:T(8,128)}, f32[128,256]{1,0:T(8,128)S(1)}, u32[]{:S(2)}) copy-start(f32[128,256]{1,0:T(8,128)S(1)} %get-tuple-element.94) | copy-start | bytes 393220
Sparse Core Ops, SparseCore 0:
  10.7 48.2 all-gather.3
  68.4 86.4 all-reduce.2
  181.0 58.9 all-gather.5
where the time goes:
time: 268 us; the launch traced here: 266 us
  waiting for transfers between devices  153 us (57%)
  matrix products  45.1 us (17%)
  local copies, waits for them, and re-layouts  28.2 us (11%)
  between operations  16.7 us (6%)
  blocking collectives  9.38 us (4%)
  starting transfers between devices  8.11 us (3%)
  other arithmetic  6.28 us (2%)
    psum x1, waiting for transfers between devices, local(): lax.psum((first_sum, second_sum, part_output, gram_query, gram_value, gra...  85.9 us
    all_gather x1, waiting for transfers between devices, one_gather(): lines, at, outs = (lax.all_gather(ravelled, axis), 0, [])  54.9 us
    dot_general x6, matrix products, across_exact(): lax.dot_general(leading, trailing, (((0,), (0,)), ((), ())), precision=la...  20.8 us
    dot_general x3, matrix products, across(): lax.dot_general(leading, trailing, (((0,), (0,)), ((), ())), preferred_el...  17 us
    all_gather x1, waiting for transfers between devices, side_by_side(): lax.all_gather(both, axis, axis=dim, tiled=True)  11.7 us
    all_to_all x1, blocking collectives, sent_to_all(): lax.all_to_all(jnp.broadcast_to(x[None], (peers, *x.shape)), axis, 0, 0,...  9.38 us
    another operation x3, local copies, waits for them, and re-layouts, in_order(): return jnp.moveaxis(pieces, 0, dim).reshape(dims)  8.26 us
    all_to_all x1, starting transfers between devices, sent_to_all(): lax.all_to_all(jnp.broadcast_to(x[None], (peers, *x.shape)), axis, 0, 0,...  7.99 us
  transfers between devices with their start and end apart: 4, of which 3 were waited for; matrix products, arithmetic and copies ran while one was open for 13% of the time, Pallas kernels for 0%

commit v1 on v0

v1 whole, which is shorter than its diff:
```python
import jax
import jax.numpy as jnp
from jax import lax
from jax.sharding import PartitionSpec as P

MODEL = 4096
CELL = 2048

beta_first = 0.8
beta_second = 0.9
floor_mean = 0.005
learn_rate = 0.05


def dot00(a, b):
    return lax.dot_general(a, b, (((0,), (0,)), ((), ())), preferred_element_type=jnp.float32)


def local(x, c, gq, gv, go, wq, wv, wo, bq, bv, bo, mq, mv, mo, sq, sv, so):
    bf = jnp.bfloat16
    f32 = jnp.float32
    bpack = jnp.concatenate(
        [jnp.concatenate([bq, bv], 1), jnp.concatenate([bo[:64], bo[64:]], 1)], 0
    )
    ball = lax.all_gather(bpack, "fs")
    wpack = jnp.concatenate(
        [jnp.concatenate([wq, wv], 1).astype(bf), wo.astype(bf)], 0
    )
    wall = lax.all_gather(wpack, "fs")
    bqv = ball[:, :256].reshape(4096, 256)
    bof = jnp.concatenate([ball[:, 256:, :128], ball[:, 256:, 128:]], 1).reshape(2048, 128)
    xb = jnp.dot(x, bqv, preferred_element_type=f32)
    cb = jnp.dot(c, bof, preferred_element_type=f32)

    def split(a):
        hi = a.astype(bf)
        return hi, (a - hi.astype(f32)).astype(bf)

    def proj(a, g):
        hi, lo = split(a)
        return dot00(hi, g) + dot00(lo, g)

    part = jnp.concatenate([proj(xb[:, :128], gq), proj(xb[:, 128:], gv), proj(cb, go)], 1)
    pieces = part.reshape(16, 8, 1024)
    mine = lax.all_to_all(pieces, "fs", 0, 0, tiled=True).sum(0)
    full = lax.all_gather(mine, "fs").reshape(128, 1024)
    mean = jnp.concatenate([mq, mv, mo], 1)
    square = jnp.concatenate([sq, sv, so], 1)
    first = beta_first * mean + (1.0 - beta_first) * full
    second = beta_second * square + (1.0 - beta_second) * full * full
    d = first / jnp.sqrt(second)
    H = lax.Precision.HIGHEST
    parts = 0.0
    for b, lo, hi in ((bqv[:, :128], 0, 256), (bqv[:, 128:], 256, 512), (bof, 512, 1024)):
        gram = dot00(b, b)
        dd = d[:, lo:hi]
        parts = parts + jnp.sum(dd * jnp.dot(gram, dd, precision=H))
    squares = lax.all_gather(parts, "tp").sum()
    factor = 1.0 / jnp.sqrt(squares / (3.0 * MODEL * CELL) + floor_mean)
    dn = -factor * d
    dq, dv, do = dn[:, :256], dn[:, 256:512], dn[:, 512:]

    def prod(b, dd):
        hi, lo = split(dd)
        return jnp.dot(b, hi, preferred_element_type=f32) + jnp.dot(b, lo, preferred_element_type=f32)

    steps = (prod(bq, dq), prod(bv, dv), prod(bo, do))

    def copy(w, b, dd):
        s = jnp.dot(b, dd.astype(bf), preferred_element_type=f32)
        return (w.astype(f32) + learn_rate * s).astype(bf)

    wqv = wall[:, :256]
    copies = (
        copy(wqv[:, :, :256].reshape(4096, 256), bqv[:, :128], dq),
        copy(wqv[:, :, 256:].reshape(4096, 256), bqv[:, 128:], dv),
        copy(wall[:, 256:].reshape(2048, 512), bof, do),
    )
    return (
        *steps,
        *copies,
        first[:, :256], first[:, 256:512], first[:, 512:],
        second[:, :256], second[:, 256:512], second[:, 512:],
    )


def solution(mesh):
    fs, both, tp = P("fs", None), P("fs", "tp"), P(None, "tp")
    in_specs = (fs, fs) + (both,) * 6 + (fs,) * 3 + (tp,) * 6
    out_specs = (both,) * 3 + (tp,) * 9
    return jax.shard_map(local, mesh=mesh, in_specs=in_specs, out_specs=out_specs, check_vma=False)
```

time: 268 us -> 173 us (0.65)
  waiting for transfers between devices: 153 us -> 53.5 us
  blocking collectives: 9.38 us -> 36.7 us
  matrix products: 45.1 us -> 28.1 us
  local copies, waits for them, and re-layouts: 28.2 us -> 20 us
  other arithmetic: 6.28 us -> 11.3 us
  starting transfers between devices: 8.11 us -> 4.71 us
    psum x1 -> x0, waiting for transfers between devices: 85.9 us -> none  [local(): lax.psum((first_sum, second_sum, part_output, gram_query, gram_value, gra...]
    all_gather x0 -> x1, blocking collectives: none -> 24 us  [local(): full = lax.all_gather(mine, 'fs').reshape(128, 1024)]
    all_gather x2, waiting for transfers between devices: 66.6 us -> 45.4 us  [the longest x1 45.4 us: local(): ball = lax.all_gather(bpack, 'fs')]
    dot_general x15 -> x23, matrix products: 45.1 us -> 28.1 us  [the longest x3 6.04 us: copy(): s = jnp.dot(b, dd.astype(bf), preferred_element_type=f32)]
    unnamed x0 -> x1, blocking collectives: none -> 12.7 us
    all_to_all x1 -> x0, blocking collectives: 9.38 us -> none  [sent_to_all(): lax.all_to_all(jnp.broadcast_to(x[None], (peers, *x.shape)), axis, 0, 0,...]
    another operation x3 -> x0, local copies, waits for them, and re-layouts: 8.26 us -> none  [in_order(): return jnp.moveaxis(pieces, 0, dim).reshape(dims)]
    slice x1 -> x8, local copies, waits for them, and re-layouts: 5.27 us -> 13.4 us  [the longest x1 2.7 us: local(): wqv[:, :, 256:].reshape(4096, 256)]
  transfers between devices with their start and end apart: 4 -> 3, of which waited for: 3 -> 2; matrix products, arithmetic and copies ran while one was open for 13% -> 25% of each run, Pallas kernels for 0% -> 0%
where the time goes in v1:
time: 173 us; the launch traced here: 171 us
  waiting for transfers between devices  53.5 us (31%)
  blocking collectives  36.7 us (21%)
  matrix products  28.1 us (16%)
  local copies, waits for them, and re-layouts  20 us (12%)
  between operations  17 us (10%)
  other arithmetic  11.3 us (7%)
  starting transfers between devices  4.71 us (3%)
    all_gather x1, waiting for transfers between devices, local(): ball = lax.all_gather(bpack, 'fs')  45.4 us
    all_gather x1, blocking collectives, local(): full = lax.all_gather(mine, 'fs').reshape(128, 1024)  24 us
    unnamed x1, blocking collectives  12.7 us
    all_to_all x1, waiting for transfers between devices, local(): mine = lax.all_to_all(pieces, 'fs', 0, 0, tiled=True).sum(0)  8.04 us
    unnamed x38, local copies, waits for them, and re-layouts  6.57 us
    dot_general x3, matrix products, copy(): s = jnp.dot(b, dd.astype(bf), preferred_element_type=f32)  6.04 us
    dot_general x1, matrix products, local(): xb = jnp.dot(x, bqv, preferred_element_type=f32)  5.98 us
    dot_general x9, matrix products, dot00(): lax.dot_general(a, b, (((0,), (0,)), ((), ())), preferred_element_type=jn...  5.16 us
  transfers between devices with their start and end apart: 3, of which 2 were waited for; matrix products, arithmetic and copies ran while one was open for 25% of the time, Pallas kernels for 0%

profile of v1, /device:TPU:0, one launch (start us, length us, event | category | flops | bytes accessed | tf_op | source)
XLA Modules:
  0.0 171.2 jit_solution(12373840907498692115)
XLA Ops:
  8.1 1.6 maximum_maximum_fusion
  14.0 45.4 %all-gather.6.cloned.1.call-done = bf16[5120,256]{1,0:T(8,128)(2,1)} async-done(((bf16[320,256]{1,0:T(8,128)(2,1)}), bf16[5120,256]{1,0:T(8,128)(2,1)}) %all-gather.6.cloned.1.call-update) | async-done | bytes 2621456 | tf_op jit(solution)/shard_map/all_gather | solution.py:25
  59.4 1.8 %slice.101 = bf16[16,256,256]{2,1,0:T(8,128)(2,1)S(1)} slice(bf16[16,320,256]{2,1,0:T(8,128)(2,1)} %bitcast.58), slice={[0:16], [0:256], [0:256]} | slice | bytes 4194304 | tf_op jit(solution)/shard_map/slice | solution.py:30
  63.0 6.0 %convolution_bitcast_fusion = f32[1024,256]{0,1:T(8,128)S(1)} fusion(bf16[4096,256]{1,0:T(8,128)(2,1)S(1)} %bitcast.47, bf16[1024,4096]{1,0:T(8,128)(2,1)} %param.17), kind=kOutput, calls=%fused_computation.8 | convolution fusion | flops 2147483648 | bytes 11534336 | tf_op jit(solution)/shard_map/dot_general | solution.py:32
  70.0 1.4 copy-done.6
  71.4 1.5 convolution_bitcast_fusion.1
  74.4 4.6 %all-to-all-start = ((f32[16,8,1024]{2,1,0:T(8,128)}), f32[16,8,1024]{2,1,0:T(8,128)}, u32[]{:S(2)}, u32[]{:S(2)}) async-start(f32[16,8,1024]{2,1,0:T(8,128)} %maximum_bitcast_fusion), calls=%async_computation | async-start | bytes 1048576 | tf_op jit(solution)/shard_map/all_to_all | solution.py:45
  79.1 2.0 %convolution_bitcast_fusion.2 = f32[128,128]{1,0:T(8,128)} fusion(bf16[16,64,128]{2,1,0:T(8,128)(2,1)} %copy-done.9, bf16[16,64,128]{2,1,0:T(8,128)(2,1)S(1)} %get-tuple-element.29), kind=kOutput, calls=%fused_computation.22 | convolution fusion | flops 68157440 | bytes 589824 | tf_op jit(solution)/shard_map/dot_general | solution.py:16
  82.7 8.0 %all-to-all-done = f32[16,8,1024]{2,1,0:T(8,128)} async-done(((f32[16,8,1024]{2,1,0:T(8,128)}), f32[16,8,1024]{2,1,0:T(8,128)}, u32[]{:S(2)}, u32[]{:S(2)}) %all-to-all-start) | async-done | bytes 524320 | tf_op jit(solution)/shard_map/all_to_all | solution.py:45
  91.8 24.0 %all-gather.1 = f32[128,1024]{1,0:T(8,128)S(1)} all-gather(f32[8,1024]{1,0:T(8,128)S(1)} %reduce_sum.45), channel_id=3, replica_groups=mesh['fs'=16,'tp'=8] {'fs'}, dimensions={0}, use_global_device_ids=true | all-gather | bytes 557056 | tf_op jit(solution)/shard_map/all_gather | solution.py:46
  115.8 2.4 %rsqrt_multiply_fusion = (f32[128,1024]{1,0:T(8,128)S(1)}, f32[128,1024]{1,0:T(8,128)}, f32[128,1024]{1,0:T(8,128)}) fusion(f32[128,1024]{1,0:T(8,128)S(1)} %all-gather.1, f32[128,512]{1,0:T(8,128)S(1)} %copy-done.13, f32[128,256]{1,0:T(8,128)} %param.32, f32[128,256]{1,0:T(8,128)} %param.31, f32[128,512]{1,0:T(8,128)} %param.30, f32[128,256]{1,0:T(8,128)} %param.29, ...), kind=kLoop, calls=%fused_computation.39 | loop fusion | flops 1572864 | bytes 3145728 | tf_op jit(solution)/shard_map/div | solution.py:51
  121.2 2.0 %fusion.14 = f32[]{:T(128)} fusion(f32[128,128]{1,0:T(8,128)} %convolution_bitcast_fusion.2, f32[128,1024]{1,0:T(8,128)} %copy-done.5), kind=kOutput, calls=%fused_computation.30 | convolution fusion | flops 100794368 | bytes 327684 | tf_op jit(solution)/shard_map/dot_general | solution.py:57
  124.6 12.7 %all-reduce = f32[8]{0:T(128)S(1)} all-reduce(f32[8]{0:T(128)S(1)} %dynamic-update-slice), channel_id=1, replica_groups=mesh['fs'=16,'tp'=8] {'tp'}, use_global_device_ids=true, to_apply=%add | all-reduce | flops 8 | bytes 64
  142.3 1.1 fusion.28
  143.5 1.1 fusion.6
  146.5 1.1 fusion.7
  148.5 1.7 slice.119
  150.2 1.7 slice.122
  151.8 1.9 %fusion.34 = (f32[128,256]{1,0:T(8,128)}, f32[128,256]{1,0:T(8,128)}, f32[128,256]{1,0:T(8,128)}, f32[128,256]{1,0:T(8,128)}) fusion(f32[128,1024]{1,0:T(8,128)} %get-tuple-element.25, f32[128,1024]{1,0:T(8,128)} %get-tuple-element.26), kind=kLoop, calls=%fused_computation.67 | loop fusion | bytes 1048576 | tf_op jit(solution)/shard_map/slice | solution.py:83
  153.7 2.7 %fusion.32 = (bf16[16,256,256]{2,1,0:T(8,128)(2,1)S(1)}, bf16[16,256,256]{2,1,0:T(8,128)(2,1)S(1)}) fusion(bf16[16,384,512]{2,1,0:T(8,128)(2,1)} %bitcast.54), kind=kLoop, calls=%fused_computation.65 | loop fusion | bytes 8388608 | tf_op jit(solution)/shard_map/slice | solution.py:76
  156.5 1.9 %slice.116 = bf16[16,128,512]{2,1,0:T(8,128)(2,1)S(1)} slice(bf16[16,384,512]{2,1,0:T(8,128)(2,1)} %bitcast.55), slice={[0:16], [256:384], [0:512]} | slice | bytes 4194304 | tf_op jit(solution)/shard_map/slice | solution.py:77
  158.3 2.0 %fusion.2 = bf16[4096,256]{1,0:T(8,128)(2,1)} fusion(bf16[4096,256]{1,0:T(8,128)(2,1)S(1)} %bitcast.53, bf16[4096,256]{1,0:T(8,128)(2,1)S(1)} %bitcast.50, f32[128,1024]{1,0:T(8,128)S(1)} %copy-done.2), kind=kOutput, calls=%fused_computation.4 | convolution fusion | flops 272629760 | bytes 5308416 | tf_op jit(solution)/shard_map/dot_general | solution.py:70
  160.3 2.0 %fusion.3 = bf16[4096,256]{1,0:T(8,128)(2,1)} fusion(bf16[4096,256]{1,0:T(8,128)(2,1)S(1)} %bitcast.52, bf16[4096,256]{1,0:T(8,128)(2,1)S(1)} %bitcast.51, f32[128,1024]{1,0:T(8,128)S(1)} %copy-done.2), kind=kOutput, calls=%fused_computation.5 | convolution fusion | flops 272629760 | bytes 5308416 | tf_op jit(solution)/shard_map/dot_general | solution.py:70
  162.4 2.0 %fusion.4 = bf16[2048,512]{1,0:T(8,128)(2,1)} fusion(bf16[2048,512]{1,0:T(8,128)(2,1)S(1)} %bitcast.46, bf16[2048,128]{1,0:T(8,128)(2,1)S(1)} %bitcast.57, f32[128,1024]{1,0:T(8,128)S(1)} %copy-done.2), kind=kOutput, calls=%fused_computation.7 | convolution fusion | flops 272629760 | bytes 4849664 | tf_op jit(solution)/shard_map/dot_general | solution.py:70
  (66 shorter events, 21.7 us)
Async XLA Ops:
  7.2 65.8 %copy-start = (bf16[1024,512]{1,0:T(8,128)(2,1)S(1)}, bf16[1024,512]{1,0:T(8,128)(2,1)}, u32[]{:S(2)}) copy-start(bf16[1024,512]{1,0:T(8,128)(2,1)} %param.21) | copy-start | bytes 3145732
  7.2 6.3 %copy-start.15 = (u32[128]{0:T(128)S(1)}, u32[128]{0:T(128)}, u32[]{:S(2)}) copy-start(u32[128]{0:T(128)} %constant.21) | copy-start | bytes 1540
  7.2 52.2 %all-gather.6.cloned.1.call-start = ((), (), s32[]{:S(2)}) async-start(), calls=%async_computation.1 | async-start | bytes 2785280 | tf_op jit(solution)/shard_map/all_gather | solution.py:25
  9.6 144.1 %all-gather.8.cloned.1.call-start = ((), (), s32[]{:S(2)}) async-start(), calls=%async_computation.2 | async-start | bytes 6684672 | tf_op jit(solution)/shard_map/all_gather | solution.py:29
  62.3 0.7 copy-start.9
  63.0 7.0 %copy-start.3 = (bf16[16,128,128]{2,1,0:T(8,128)(2,1)}, bf16[16,128,128]{2,1,0:T(8,128)(2,1)S(1)}, u32[]{:S(2)}) copy-start(bf16[16,128,128]{2,1,0:T(8,128)(2,1)S(1)} %pad_maximum_fusion) | copy-start | bytes 1572868
  63.0 6.0 %copy-start.7 = (bf16[1024,256]{1,0:T(8,128)(2,1)S(1)}, bf16[1024,256]{1,0:T(8,128)(2,1)}, u32[]{:S(2)}) copy-start(bf16[1024,256]{1,0:T(8,128)(2,1)} %param.19) | copy-start | bytes 1572868
  63.0 6.3 %copy-start.8 = (bf16[1024,256]{1,0:T(8,128)(2,1)S(1)}, bf16[1024,256]{1,0:T(8,128)(2,1)}, u32[]{:S(2)}) copy-start(bf16[1024,256]{1,0:T(8,128)(2,1)} %param.20) | copy-start | bytes 1572868
  69.0 2.4 %copy-start.6 = (bf16[1024,2048]{1,0:T(8,128)(2,1)S(1)}, bf16[1024,2048]{1,0:T(8,128)(2,1)}, u32[]{:S(2)}) copy-start(bf16[1024,2048]{1,0:T(8,128)(2,1)} %param.18) | copy-start | bytes 12582916
  74.4 16.3 %all-to-all-start = ((f32[16,8,1024]{2,1,0:T(8,128)}), f32[16,8,1024]{2,1,0:T(8,128)}, u32[]{:S(2)}, u32[]{:S(2)}) async-start(f32[16,8,1024]{2,1,0:T(8,128)} %maximum_bitcast_fusion), calls=%async_computation | async-start | bytes 1048576 | tf_op jit(solution)/shard_map/all_to_all | solution.py:45
  81.1 34.7 %copy-start.13 = (f32[128,512]{1,0:T(8,128)S(1)}, f32[128,512]{1,0:T(8,128)}, u32[]{:S(2)}) copy-start(f32[128,512]{1,0:T(8,128)} %param.33) | copy-start | bytes 786436
  91.8 27.2 %copy-start.14 = (f32[128,128]{1,0:T(8,128)S(1)}, f32[128,128]{1,0:T(8,128)}, u32[]{:S(2)}) copy-start(f32[128,128]{1,0:T(8,128)} %fusion.12) | copy-start | bytes 196612
  91.8 47.9 %copy-start.12 = (bf16[128,128]{1,0:T(8,128)(2,1)S(1)}, bf16[128,128]{1,0:T(8,128)(2,1)}, u32[]{:S(2)}) copy-start(bf16[128,128]{1,0:T(8,128)(2,1)} %param.27) | copy-start | bytes 98308
  118.1 0.9 copy-start.5
  118.1 24.2 %copy-start.10 = (bf16[256,128]{1,0:T(8,128)(2,1)S(1)}, bf16[256,128]{1,0:T(8,128)(2,1)}, u32[]{:S(2)}) copy-start(bf16[256,128]{1,0:T(8,128)(2,1)} %param.26) | copy-start | bytes 196612
  119.0 26.4 %copy-start.11 = (bf16[256,128]{1,0:T(8,128)(2,1)S(1)}, bf16[256,128]{1,0:T(8,128)(2,1)}, u32[]{:S(2)}) copy-start(bf16[256,128]{1,0:T(8,128)(2,1)} %param.25) | copy-start | bytes 196612
  139.7 0.8 copy-start.1
  156.4 1.9 %copy-start.2 = (f32[128,1024]{1,0:T(8,128)S(1)}, f32[128,1024]{1,0:T(8,128)}, u32[]{:S(2)}) copy-start(f32[128,1024]{1,0:T(8,128)} %copy-done.1) | copy-start | bytes 1572868
  160.3 2.0 %copy-start.4 = (bf16[16,128,128]{2,1,0:T(8,128)(2,1)S(1)}, bf16[16,128,128]{2,1,0:T(8,128)(2,1)}, u32[]{:S(2)}) copy-start(bf16[16,128,128]{2,1,0:T(8,128)(2,1)} %copy-done.3) | copy-start | bytes 1572868
Sparse Core Ops, SparseCore 0:
  10.7 48.6 all-gather.5
  61.6 66.6 all-gather.7

commit v2 on v1

v2 whole, which is shorter than its diff:
```python
import functools

import jax
import jax.numpy as jnp
from jax import lax
from jax.experimental import pallas as pl
from jax.experimental.pallas import tpu as pltpu
from jax.sharding import PartitionSpec as P

MODEL = 4096
CELL = 2048

beta_first = 0.8
beta_second = 0.9
floor_mean = 0.005
learn_rate = 0.05

f32 = jnp.float32
bf16 = jnp.bfloat16
HIGH = lax.Precision.HIGHEST
SIDE = 4
FS = SIDE * SIDE
TP = 8
B_ROWS = 320
W_ROWS = 384
B_CUTS = ((0, 48), (48, 32), (80, 48), (128, 32))
W_CUTS = ((0, 96), (96, 96), (192, 96), (288, 96))
OTHERS = [(dz, dx) for dz in range(SIDE) for dx in range(SIDE) if dz or dx]
MESH = pl.DeviceIdType.MESH


def slot(dz, dx):
    return (dz % SIDE) * SIDE + dx % SIDE


def link_plan(along_x, sign):
    near, far = ((0, 1), (2, 3)) if along_x else ((2, 3), (0, 1))
    which = 0 if sign > 0 else 1

    def at(far_off, near_off):
        return (far_off, near_off) if along_x else (near_off, far_off)

    steps = [(at(0, 0), near[0]), (at(0, 0), near[1]), (at(0, 0), far[0]), (at(0, 0), far[1])]
    steps.append((at(0, -sign), near[which]))
    steps += [(at(-1, 0), far[0]), (at(-1, 0), far[1]), (at(1, 0), far[0]), (at(1, 0), far[1])]
    steps.append((at(0, -sign), far[which]))
    steps += [(at(2, 0), far[0]), (at(2, 0), far[1])]
    steps += [(at(-1, -sign), far[which]), (at(1, -sign), far[which]), (at(2, -sign), far[which])]
    return steps


LINKS = [(True, 1), (True, -1), (False, 1), (False, -1)]
PLANS = [link_plan(*link) for link in LINKS]
STEPS = 15


def dot00(a, b):
    return lax.dot_general(a, b, (((0,), (0,)), ((), ())), preferred_element_type=f32)


def dot(a, b):
    return jnp.dot(a, b, preferred_element_type=f32)


class Torus:
    def __init__(self, buf, rows, send, recv, blk, neighbour):
        self.buf, self.rows, self.send, self.recv = buf, rows, send, recv
        self.blk, self.neighbour = blk, neighbour
        self.seen, self.started = set(), []

    def view(self, off, piece):
        start, size = self.rows[piece]
        return self.buf.at[self.blk(*off), pl.ds(start, size), :]

    def copy(self, off, piece, link, step, dest_off):
        ref = self.view(off, piece)
        return pltpu.make_async_remote_copy(
            src_ref=ref,
            dst_ref=ref,
            send_sem=self.send.at[link * STEPS + step],
            recv_sem=self.recv.at[slot(*dest_off) * 4 + piece],
            device_id={"fs": self.neighbour[link]},
            device_id_type=MESH,
        )

    def need(self, off, piece):
        off = (off[0] % SIDE, off[1] % SIDE)
        if off == (0, 0) or (off, piece) in self.seen:
            return
        self.seen.add((off, piece))
        ref = self.view(off, piece)
        pltpu.make_async_remote_copy(
            src_ref=ref,
            dst_ref=ref,
            send_sem=self.send.at[0],
            recv_sem=self.recv.at[slot(*off) * 4 + piece],
            device_id={"fs": self.neighbour[0]},
            device_id_type=MESH,
        ).wait_recv()

    def step(self, s):
        for link, (along_x, sign) in enumerate(LINKS):
            off, piece = PLANS[link][s]
            self.need(off, piece)
            dest = (off[0], off[1] - sign) if along_x else (off[0] - sign, off[1])
            c = self.copy(off, piece, link, s, dest)
            c.start()
            self.started.append(c)

    def block(self, off):
        for piece in range(4):
            self.need(off, piece)

    def finish(self):
        for c in self.started:
            c.wait_send()


def gather_kernel(
    x_h, c_h, gq_h, gv_h, go_h, wq_h, wv_h, wo_h, bq_h, bv_h, bo_h,
    mq_h, mv_h, mo_h, sq_h, sv_h, so_h,
    wall, ball, dcopy, stq, stv, sto, f1q, f1v, f1o, f2q, f2v, f2o,
    x, c, gq, gv, go, wqv, wo, mean, square,
    xb, cb, hl, part, psend, precv, pall, gram, d, sqs,
    lsem, wsend, wrecv, bsend, brecv, psems, psemr, rsend, rrecv, asend, arecv, ssend, srecv,
):
    f = lax.axis_index("fs")
    t = lax.axis_index("tp")
    z, xx = f // SIDE, lax.rem(f, SIDE)
    core = lax.rem(t, 2)

    def blk(dz, dx):
        return lax.rem(z + (dz % SIDE), SIDE) * SIDE + lax.rem(xx + (dx % SIDE), SIDE)

    n = [0]

    def load(src, dst):
        cp = pltpu.make_async_copy(src, dst, lsem.at[n[0]])
        n[0] += 1
        cp.start()
        return cp

    base_in = [
        load(bq_h, ball.at[f, pl.ds(0, 256), pl.ds(0, 128)]),
        load(bv_h, ball.at[f, pl.ds(0, 256), pl.ds(128, 128)]),
        load(bo_h.at[pl.ds(0, 64), :], ball.at[f, pl.ds(256, 64), pl.ds(0, 128)]),
        load(bo_h.at[pl.ds(64, 64), :], ball.at[f, pl.ds(256, 64), pl.ds(128, 128)]),
    ]
    w_in = [
        load(wq_h, wqv.at[:, pl.ds(0, 256)]),
        load(wv_h, wqv.at[:, pl.ds(256, 256)]),
        load(wo_h, wo),
    ]
    x_in = [load(x_h, x), load(c_h, c)]
    g_in = [load(gq_h, gq), load(gv_h, gv), load(go_h, go)]
    m_in = [
        load(mq_h, mean.at[:, pl.ds(0, 256)]),
        load(mv_h, mean.at[:, pl.ds(256, 256)]),
        load(mo_h, mean.at[:, pl.ds(512, 512)]),
        load(sq_h, square.at[:, pl.ds(0, 256)]),
        load(sv_h, square.at[:, pl.ds(256, 256)]),
        load(so_h, square.at[:, pl.ds(512, 512)]),
    ]

    barrier = pltpu.get_barrier_semaphore()
    for off in OTHERS:
        pl.semaphore_signal(barrier, inc=1, device_id={"fs": blk(*off)}, device_id_type=MESH)
    for r in range(1, TP):
        pl.semaphore_signal(
            barrier, inc=1, device_id={"tp": lax.rem(t + r, TP)}, device_id_type=MESH
        )
    for cp in w_in:
        cp.wait()
    wall[f, 0:256, :] = wqv[...].astype(bf16)
    wall[f, 256:384, :] = wo[...].astype(bf16)
    for cp in base_in:
        cp.wait()
    pl.semaphore_wait(barrier, FS - 1 + TP - 1)

    neighbour = [blk(0, 1), blk(0, -1), blk(1, 0), blk(-1, 0)]
    half = pl.multiple_of(core * 160, 16)
    brows = [(pl.multiple_of(half + start, 16), size) for start, size in B_CUTS]
    bases = Torus(ball, brows, bsend, brecv, blk, neighbour)
    weights = Torus(wall, W_CUTS, wsend, wrecv, blk, neighbour)

    other = t + 1 - 2 * core
    passed = []

    def partner(off, start):
        rows = pl.ds(pl.multiple_of(start * 160, 16), 160)
        ref = ball.at[blk(*off), rows, :]
        return pltpu.make_async_remote_copy(
            src_ref=ref,
            dst_ref=ref,
            send_sem=psems.at[slot(*off)],
            recv_sem=psemr.at[slot(*off)],
            device_id={"tp": other},
            device_id_type=MESH,
        )

    def hand_over(offs):
        for off in offs:
            bases.block(off)
            cp = partner(off, core)
            cp.start()
            passed.append(cp)

    def project(offs, first=False):
        for off in offs:
            b = blk(*off)
            if off != (0, 0):
                partner(off, 1 - core).wait_recv()
            xc = pl.ds(pl.multiple_of(b * 256, 256), 256)
            cc = pl.ds(pl.multiple_of(b * 128, 128), 128)
            bo = jnp.concatenate([ball[b, 256:320, 0:128], ball[b, 256:320, 128:256]], axis=0)
            px = dot(x[:, xc], ball[b, 0:256, :])
            pc = dot(c[:, cc], bo)
            if first and off == offs[0]:
                xb[...] = px
                cb[...] = pc
            else:
                xb[...] += px
                cb[...] += pc

    near = [(0, 1), (0, -1), (1, 0), (-1, 0)]
    middle = [(-1, -1), (-1, 1), (1, -1), (1, 1), (0, 2), (2, 0)]
    last = [(-1, 2), (1, 2), (2, -1), (2, 1), (2, 2)]

    for s in range(4):
        bases.step(s)
    weights.step(0)
    for s in range(4, 10):
        bases.step(s)
    hand_over(near)
    for cp in x_in:
        cp.wait()
    project([(0, 0)], first=True)
    project(near)
    for s in range(10, 14):
        bases.step(s)
    hand_over(middle)
    bases.step(14)
    weights.step(1)
    weights.step(2)
    project(middle)
    hand_over(last)
    weights.step(3)
    project(last)

    for cp in g_in:
        cp.wait()

    def split(a, at):
        hi = a.astype(bf16)
        hl[:, at : at + 128] = hi
        hl[:, at + 128 : at + 256] = (a - hi.astype(f32)).astype(bf16)

    split(xb[:, 0:128], 0)
    split(xb[:, 128:256], 256)
    split(cb[...], 512)
    for at, g, lo, hi in ((0, gq, 0, 256), (256, gv, 256, 512), (512, go, 512, 1024)):
        both = dot00(hl[:, at : at + 256], g[...])
        part[:, lo:hi] = both[0:128] + both[128:256]
    for j in range(FS):
        r, cc = 16 * (j // 2), 512 * (j % 2)
        psend[j] = part[r : r + 16, cc : cc + 512].astype(bf16)

    gq_sum = jnp.zeros((256, 256), f32)
    go_sum = jnp.zeros((128, 128), f32)
    for j in range(FS):
        bqv = ball[j, 0:256, :]
        bo = jnp.concatenate([ball[j, 256:320, 0:128], ball[j, 256:320, 128:256]], axis=0)
        gq_sum += dot00(bqv, bqv)
        go_sum += dot00(bo, bo)
    gram[0] = gq_sum[0:128, 0:128]
    gram[1] = gq_sum[128:256, 128:256]
    gram[2] = go_sum

    def to_peer(src, dst, send, recv, off):
        return pltpu.make_async_remote_copy(
            src_ref=src,
            dst_ref=dst,
            send_sem=send.at[slot(*off)],
            recv_sem=recv.at[slot(-off[0], -off[1])],
            device_id={"fs": blk(*off)},
            device_id_type=MESH,
        )

    scattered = []
    for off in OTHERS:
        cp = to_peer(psend.at[blk(*off)], precv.at[f], rsend, rrecv, off)
        cp.start()
        scattered.append(cp)
    weights.step(4)
    precv[f] = psend[f]
    for off in OTHERS:
        b = blk(*off)
        to_peer(psend.at[b], precv.at[b], rsend, rrecv, (-off[0], -off[1])).wait_recv()
    total = precv[0].astype(f32)
    for j in range(1, FS):
        total += precv[j].astype(f32)
    pall[f] = total.astype(bf16)
    weights.step(5)
    gathered = []
    for off in OTHERS:
        cp = to_peer(pall.at[f], pall.at[f], asend, arecv, off)
        cp.start()
        gathered.append(cp)
    weights.step(6)
    weights.step(7)
    for cp in m_in:
        cp.wait()
    for off in OTHERS:
        b = blk(*off)
        to_peer(pall.at[b], pall.at[b], asend, arecv, (-off[0], -off[1])).wait_recv()

    for j in range(FS):
        r, cc = 16 * (j // 2), 512 * (j % 2)
        rows = slice(r, r + 16)
        p = pall[j].astype(f32)
        one = beta_first * mean[rows, cc : cc + 512] + (1.0 - beta_first) * p
        two = beta_second * square[rows, cc : cc + 512] + (1.0 - beta_second) * p * p
        if j % 2:
            f1o[rows, :] = one
            f2o[rows, :] = two
        else:
            f1q[rows, :] = one[:, 0:256]
            f1v[rows, :] = one[:, 256:512]
            f2q[rows, :] = two[:, 0:256]
            f2v[rows, :] = two[:, 256:512]
        d[rows, cc : cc + 512] = one / jnp.sqrt(two)

    sums = jnp.zeros((1, 1), f32)
    for i, (lo, hi) in enumerate(((0, 256), (256, 512), (512, 1024))):
        dd = d[:, lo:hi]
        gd = jnp.dot(gram[i], dd, precision=HIGH, preferred_element_type=f32)
        sums += jnp.sum(dd * gd, keepdims=True)
    sqs[t] = jnp.broadcast_to(sums, (8, 128))
    weights.step(8)
    weights.step(9)

    def to_tp(src, r):
        return pltpu.make_async_remote_copy(
            src_ref=src,
            dst_ref=src,
            send_sem=ssend.at[r],
            recv_sem=srecv.at[(-r) % TP],
            device_id={"tp": lax.rem(t + r, TP)},
            device_id_type=MESH,
        )

    summed = []
    for r in range(1, TP):
        cp = to_tp(sqs.at[t], r)
        cp.start()
        summed.append(cp)
    weights.step(10)
    for r in range(1, TP):
        to_tp(sqs.at[lax.rem(t + r, TP)], TP - r).wait_recv()
    squares = sqs[0]
    for i in range(1, TP):
        squares += sqs[i]
    factor = 1.0 / jnp.sqrt(squares[0:1, 0:1] / (3.0 * MODEL * CELL) + floor_mean)
    dn = -factor * d[...]
    dcopy[...] = (learn_rate * dn).astype(bf16)
    weights.step(11)
    hi = dn.astype(bf16)
    lo = (dn - hi.astype(f32)).astype(bf16)
    bq = ball[f, 0:256, 0:128]
    bv = ball[f, 0:256, 128:256]
    bo = jnp.concatenate([ball[f, 256:320, 0:128], ball[f, 256:320, 128:256]], axis=0)
    stq[...] = dot(bq, hi[:, 0:256]) + dot(bq, lo[:, 0:256])
    stv[...] = dot(bv, hi[:, 256:512]) + dot(bv, lo[:, 256:512])
    sto[...] = dot(bo, hi[:, 512:1024]) + dot(bo, lo[:, 512:1024])
    for s in range(12, 15):
        weights.step(s)
    for off in OTHERS:
        weights.block(off)
    bases.finish()
    weights.finish()
    for cp in passed + scattered + gathered + summed:
        cp.wait_send()


def finish_kernel(
    wall, ball, dcopy, stq, stv, sto, f1q, f1v, f1o, f2q, f2v, f2o,
    o_stq, o_stv, o_sto, o_q, o_v, o_o, o_f1q, o_f1v, o_f1o, o_f2q, o_f2v, o_f2o,
    cq, cv, co, sem, csem,
):
    plain = [
        pltpu.make_async_copy(src, dst, sem.at[i])
        for i, (src, dst) in enumerate(
            (
                (stq, o_stq), (stv, o_stv), (sto, o_sto), (f1q, o_f1q), (f1v, o_f1v),
                (f1o, o_f1o), (f2q, o_f2q), (f2v, o_f2v), (f2o, o_f2o),
            )
        )
    ]
    for cp in plain:
        cp.start()
    sent = []
    for k in range(FS):
        bo = jnp.concatenate([ball[k, 256:320, 0:128], ball[k, 256:320, 128:256]], axis=0)
        wq = wall[k, 0:256, 0:256].astype(f32)
        cq[k * 256 : k * 256 + 256, :] = (
            wq + dot(ball[k, 0:256, 0:128], dcopy[:, 0:256])
        ).astype(bf16)
        wv = wall[k, 0:256, 256:512].astype(f32)
        cv[k * 256 : k * 256 + 256, :] = (
            wv + dot(ball[k, 0:256, 128:256], dcopy[:, 256:512])
        ).astype(bf16)
        wo = wall[k, 256:384, :].astype(f32)
        co[k * 128 : k * 128 + 128, :] = (wo + dot(bo, dcopy[:, 512:1024])).astype(bf16)
        for i, (src, dst, n) in enumerate(((cq, o_q, 256), (cv, o_v, 256), (co, o_o, 128))):
            cp = pltpu.make_async_copy(
                src.at[pl.ds(k * n, n), :], dst.at[pl.ds(k * n, n), :], csem.at[k * 3 + i]
            )
            cp.start()
            sent.append(cp)
    for cp in plain + sent:
        cp.wait()


def local(*args):
    tokens = args[0].shape[0]
    any_spec = pl.BlockSpec(memory_space=pl.ANY)
    vmem_spec = pl.BlockSpec(memory_space=pltpu.VMEM)
    mids = [
        ((FS, W_ROWS, 512), bf16),
        ((FS, B_ROWS, 256), bf16),
        ((128, 1024), bf16),
        ((256, 256), f32),
        ((256, 256), f32),
        ((128, 512), f32),
        ((128, 256), f32),
        ((128, 256), f32),
        ((128, 512), f32),
        ((128, 256), f32),
        ((128, 256), f32),
        ((128, 512), f32),
    ]
    dma = pltpu.SemaphoreType.DMA
    mid = pl.pallas_call(
        gather_kernel,
        out_shape=[pltpu.VMEM(s, t) for s, t in mids],
        in_specs=[any_spec] * 17,
        out_specs=[vmem_spec] * len(mids),
        scratch_shapes=[
            pltpu.VMEM((tokens, MODEL), bf16),
            pltpu.VMEM((tokens, CELL), bf16),
            pltpu.VMEM((tokens, 256), bf16),
            pltpu.VMEM((tokens, 256), bf16),
            pltpu.VMEM((tokens, 512), bf16),
            pltpu.VMEM((256, 512), f32),
            pltpu.VMEM((128, 512), f32),
            pltpu.VMEM((128, 1024), f32),
            pltpu.VMEM((128, 1024), f32),
            pltpu.VMEM((tokens, 256), f32),
            pltpu.VMEM((tokens, 128), f32),
            pltpu.VMEM((tokens, 768), bf16),
            pltpu.VMEM((128, 1024), f32),
            pltpu.VMEM((FS, 16, 512), bf16),
            pltpu.VMEM((FS, 16, 512), bf16),
            pltpu.VMEM((FS, 16, 512), bf16),
            pltpu.VMEM((3, 128, 128), f32),
            pltpu.VMEM((128, 1024), f32),
            pltpu.VMEM((TP, 8, 128), f32),
            dma((18,)),
            dma((60,)), dma((64,)), dma((60,)), dma((64,)), dma((16,)), dma((16,)),
            dma((16,)), dma((16,)), dma((16,)), dma((16,)), dma((8,)), dma((8,)),
        ],
        compiler_params=pltpu.CompilerParams(
            collective_id=0, has_side_effects=True, vmem_limit_bytes=48 * 1024 * 1024
        ),
        name="gather_and_reduce",
    )(*args)
    outs = [
        ((256, 256), f32), ((256, 256), f32), ((128, 512), f32),
        ((MODEL, 256), bf16), ((MODEL, 256), bf16), ((CELL, 512), bf16),
        ((128, 256), f32), ((128, 256), f32), ((128, 512), f32),
        ((128, 256), f32), ((128, 256), f32), ((128, 512), f32),
    ]
    return tuple(
        pl.pallas_call(
            finish_kernel,
            out_shape=[jax.ShapeDtypeStruct(s, t) for s, t in outs],
            in_specs=[vmem_spec] * len(mids),
            out_specs=[any_spec] * len(outs),
            scratch_shapes=[
                pltpu.VMEM((MODEL, 256), bf16),
                pltpu.VMEM((MODEL, 256), bf16),
                pltpu.VMEM((CELL, 512), bf16),
                dma((9,)),
                dma((48,)),
            ],
            compiler_params=pltpu.CompilerParams(vmem_limit_bytes=40 * 1024 * 1024),
            name="write_copies",
        )(*mid)
    )


def solution(mesh):
    fs, both, tp = P("fs", None), P("fs", "tp"), P(None, "tp")
    in_specs = (fs, fs) + (both,) * 6 + (fs,) * 3 + (tp,) * 6
    out_specs = (both,) * 3 + (tp,) * 9
    return jax.shard_map(local, mesh=mesh, in_specs=in_specs, out_specs=out_specs, check_vma=False)
```

time: 173 us -> 72.3 us (0.42)
  Pallas kernels: 0 us -> 65.7 us
  waiting for transfers between devices: 53.5 us -> 0 us
  blocking collectives: 36.7 us -> 0 us
  matrix products: 28.1 us -> 0 us
  between operations: 17 us -> 0.67 us
  local copies, waits for them, and re-layouts: 20 us -> 5.42 us
  other arithmetic: 11.3 us -> 0 us
  starting transfers between devices: 4.71 us -> 0 us
    pallas_call x0 -> x2, Pallas kernels: none -> 65.7 us  [the longest x1 61.8 us: local(): pl.pallas_call(gather_kernel, out_shape=[pltpu.VMEM(s, t) for s, t in mid...]
    all_gather x2 -> x0, waiting for transfers between devices: 45.4 us -> none  [the longest x1 45.4 us: local(): ball = lax.all_gather(bpack, 'fs')]
    dot_general x23 -> x0, matrix products: 28.1 us -> none  [the longest x3 6.04 us: copy(): s = jnp.dot(b, dd.astype(bf), preferred_element_type=f32)]
    all_gather x1 -> x0, blocking collectives: 24 us -> none  [local(): full = lax.all_gather(mine, 'fs').reshape(128, 1024)]
    slice x8 -> x0, local copies, waits for them, and re-layouts: 13.4 us -> none  [the longest x1 2.7 us: local(): wqv[:, :, 256:].reshape(4096, 256)]
    unnamed x1 -> x0, blocking collectives: 12.7 us -> none
    all_to_all x1 -> x0, waiting for transfers between devices: 8.04 us -> none  [local(): mine = lax.all_to_all(pieces, 'fs', 0, 0, tiled=True).sum(0)]
    all_to_all x1 -> x0, starting transfers between devices: 4.62 us -> none  [local(): mine = lax.all_to_all(pieces, 'fs', 0, 0, tiled=True).sum(0)]
  transfers between devices with their start and end apart: 3 -> 0, of which waited for: 2 -> 0; matrix products, arithmetic and copies ran while one was open for 25% -> 0% of each run, Pallas kernels for 0% -> 0%
where the time goes in v2:
time: 72.3 us; the launch traced here: 71.8 us
  Pallas kernels  65.7 us (91%)
  local copies, waits for them, and re-layouts  5.42 us (7%)
    pallas_call x1, Pallas kernels, local(): pl.pallas_call(gather_kernel, out_shape=[pltpu.VMEM(s, t) for s, t in mid...  61.8 us
    unnamed x4, local copies, waits for them, and re-layouts  5.42 us
    pallas_call x1, Pallas kernels, local(): pl.pallas_call(finish_kernel, out_shape=[jax.ShapeDtypeStruct(s, t) for s...  3.87 us

profile of v2, /device:TPU:0, one launch (start us, length us, event | category | flops | bytes accessed | tf_op | source)
XLA Modules:
  0.0 71.8 jit_solution(18288864735671418613)
XLA Ops:
  0.7 61.8 %gather_and_reduce.1 = (bf16[16,384,512]{2,1,0:T(8,128)(2,1)S(1)}, bf16[16,320,256]{2,1,0:T(8,128)(2,1)S(1)}, bf16[128,1024]{1,0:T(8,128)(2,1)S(1)}, f32[256,256...) custom-call(bf16[1024,4096]{1,0:T(8,128)(2,1)} %x_h.1, ...), custom_call_target="tpu_custom_call" | custom-call | tf_op jit(solution)/shard_map/gather_and_reduce/pallas_call | solution.py:443
  62.5 0.0 copy-start
  62.5 2.6 %copy-done = bf16[16,384,512]{2,1,0:T(8,128)(2,1)} copy-done((bf16[16,384,512]{2,1,0:T(8,128)(2,1)}, bf16[16,384,512]{2,1,0:T(8,128)(2,1)S(1)}, u32[]{:S(2)}) %copy-start) | copy-done | bytes 6291480
  65.1 0.0 copy-start.1
  65.1 2.8 %copy-done.1 = bf16[16,384,512]{2,1,0:T(8,128)(2,1)S(1)} copy-done((bf16[16,384,512]{2,1,0:T(8,128)(2,1)S(1)}, bf16[16,384,512]{2,1,0:T(8,128)(2,1)}, u32[]{:S(2)}) %copy-start.1) | copy-done | bytes 6291480
  67.9 3.9 %write_copies.1 = (f32[256,256]{1,0:T(8,128)}, f32[256,256]{1,0:T(8,128)}, f32[128,512]{1,0:T(8,128)}, bf16[4096,256]{1,0:T(8,128)(2,1)}, bf16[4096,256]{1,0:T(8...) custom-call(bf16[16,384,512]{2,1,0:T(8,128)(2,1)S(1)} %copy-done.1, ...), custom_call_target="tpu_custom_call" | custom-call | tf_op jit(solution)/shard_map/write_copies/pallas_call | solution.py:484
Async XLA Ops:
  62.5 2.6 %copy-start = (bf16[16,384,512]{2,1,0:T(8,128)(2,1)}, bf16[16,384,512]{2,1,0:T(8,128)(2,1)S(1)}, u32[]{:S(2)}) copy-start(bf16[16,384,512]{2,1,0:T(8,128)(2,1)S(1)} %get-tuple-element.24.wall) | copy-start | bytes 18874372
  65.1 2.8 %copy-start.1 = (bf16[16,384,512]{2,1,0:T(8,128)(2,1)S(1)}, bf16[16,384,512]{2,1,0:T(8,128)(2,1)}, u32[]{:S(2)}) copy-start(bf16[16,384,512]{2,1,0:T(8,128)(2,1)} %copy-done) | copy-start | bytes 18874372

commit v3 on v2

--- a/solution.py
+++ b/solution.py
@@ -23,9 +23,12 @@
 TP = 8
 B_ROWS = 320
 W_ROWS = 384
-B_CUTS = ((0, 48), (48, 32), (80, 48), (128, 32))
+SLICE = B_ROWS // TP
 W_CUTS = ((0, 96), (96, 96), (192, 96), (288, 96))
-OTHERS = [(dz, dx) for dz in range(SIDE) for dx in range(SIDE) if dz or dx]
+NEAR = [(0, 1), (0, -1), (1, 0), (-1, 0)]
+MIDDLE = [(-1, -1), (-1, 1), (1, -1), (1, 1), (0, 2), (2, 0)]
+FAR = [(-1, 2), (1, 2), (2, -1), (2, 1), (2, 2)]
+OTHERS = NEAR + MIDDLE + FAR
 MESH = pl.DeviceIdType.MESH
 
 
@@ -122,7 +125,7 @@
     wall, ball, dcopy, stq, stv, sto, f1q, f1v, f1o, f2q, f2v, f2o,
     x, c, gq, gv, go, wqv, wo, mean, square,
     xb, cb, hl, part, psend, precv, pall, gram, d, sqs,
-    lsem, wsend, wrecv, bsend, brecv, psems, psemr, rsend, rrecv, asend, arecv, ssend, srecv,
+    lsem, wsend, wrecv, bsend, brecv, psems, psemr, ysend, yrecv, rsend, rrecv, asend, arecv, ssend, srecv,
 ):
     f = lax.axis_index("fs")
     t = lax.axis_index("tp")
@@ -178,74 +181,119 @@
     pl.semaphore_wait(barrier, FS - 1 + TP - 1)
 
     neighbour = [blk(0, 1), blk(0, -1), blk(1, 0), blk(-1, 0)]
-    half = pl.multiple_of(core * 160, 16)
-    brows = [(pl.multiple_of(half + start, 16), size) for start, size in B_CUTS]
-    bases = Torus(ball, brows, bsend, brecv, blk, neighbour)
     weights = Torus(wall, W_CUTS, wsend, wrecv, blk, neighbour)
-
-    other = t + 1 - 2 * core
-    passed = []
-
-    def partner(off, start):
-        rows = pl.ds(pl.multiple_of(start * 160, 16), 160)
+    y = t // 2
+    above, below = lax.rem(y + 1, SIDE), lax.rem(y + SIDE - 1, SIDE)
+    copies = []
+
+    def slice_rows(level, start, size):
+        return pl.ds(pl.multiple_of((core * SIDE + level) * SLICE + start, 8), size)
+
+    def spread(off, send_at, recv_at, rows, device_id, send, recv):
         ref = ball.at[blk(*off), rows, :]
         return pltpu.make_async_remote_copy(
             src_ref=ref,
             dst_ref=ref,
-            send_sem=psems.at[slot(*off)],
-            recv_sem=psemr.at[slot(*off)],
-            device_id={"tp": other},
+            send_sem=send.at[send_at],
+            recv_sem=recv.at[recv_at],
+            device_id=device_id,
             device_id_type=MESH,
         )
 
+    def start(cp):
+        cp.start()
+        copies.append(cp)
+
+    def in_plane(off, src, arriving):
+        return spread(
+            src, slot(*off), slot(*arriving), slice_rows(y, 0, SLICE), {"fs": blk(*off)}, bsend, brecv
+        )
+
+    def level(kind, off, y_of, cut, up):
+        i = kind * FS + slot(*off)
+        tp_at = (above if up else below) * 2 + core
+        return spread(off, i, i, slice_rows(y_of, *cut), {"tp": tp_at}, ysend, yrecv)
+
+    def cuts(off):
+        half = 24 if OTHERS.index(off) % 2 else 16
+        return (0, half), (half, SLICE - half)
+
+    def send_levels(offs):
+        for off in offs:
+            in_plane(off, off, off).wait_recv()
+            start(level(0, off, y, (0, SLICE), True))
+            start(level(1, off, y, (0, SLICE), False))
+
+    def relay_levels(offs):
+        for off in offs:
+            low, high = cuts(off)
+            level(0, off, below, (0, SLICE), True).wait_recv()
+            start(level(2, off, below, low, True))
+            level(1, off, above, (0, SLICE), False).wait_recv()
+            start(level(3, off, above, high, False))
+
+    def partner(off, of_core):
+        rows = pl.ds(pl.multiple_of(of_core * SIDE * SLICE, 8), SIDE * SLICE)
+        i = slot(*off)
+        return spread(off, i, i, rows, {"tp": t + 1 - 2 * core}, psems, psemr)
+
     def hand_over(offs):
+        opposite = lax.rem(y + 2, SIDE)
         for off in offs:
-            bases.block(off)
-            cp = partner(off, core)
-            cp.start()
-            passed.append(cp)
+            low, high = cuts(off)
+            level(2, off, opposite, low, True).wait_recv()
+            level(3, off, opposite, high, False).wait_recv()
+            start(partner(off, core))
+
+    def outputs_of(b):
+        return jnp.concatenate([ball[b, 256:320, 0:128], ball[b, 256:320, 128:256]], axis=0)
 
     def project(offs, first=False):
+        bs = [blk(*off) for off in offs]
         for off in offs:
-            b = blk(*off)
             if off != (0, 0):
                 partner(off, 1 - core).wait_recv()
-            xc = pl.ds(pl.multiple_of(b * 256, 256), 256)
-            cc = pl.ds(pl.multiple_of(b * 128, 128), 128)
-            bo = jnp.concatenate([ball[b, 256:320, 0:128], ball[b, 256:320, 128:256]], axis=0)
-            px = dot(x[:, xc], ball[b, 0:256, :])
-            pc = dot(c[:, cc], bo)
-            if first and off == offs[0]:
-                xb[...] = px
-                cb[...] = pc
-            else:
-                xb[...] += px
-                cb[...] += pc
-
-    near = [(0, 1), (0, -1), (1, 0), (-1, 0)]
-    middle = [(-1, -1), (-1, 1), (1, -1), (1, 1), (0, 2), (2, 0)]
-    last = [(-1, 2), (1, 2), (2, -1), (2, 1), (2, 2)]
-
+        xs = [x[:, pl.ds(pl.multiple_of(b * 256, 256), 256)] for b in bs]
+        cs = [c[:, pl.ds(pl.multiple_of(b * 128, 128), 128)] for b in bs]
+        px = dot(
+            jnp.concatenate(xs, axis=1), jnp.concatenate([ball[b, 0:256, :] for b in bs], axis=0)
+        )
+        pc = dot(jnp.concatenate(cs, axis=1), jnp.concatenate([outputs_of(b) for b in bs], axis=0))
+        if first:
+            xb[...] = px
+            cb[...] = pc
+        else:
+            xb[...] += px
+            cb[...] += pc
+
+    for off in OTHERS:
+        start(in_plane(off, (0, 0), (-off[0], -off[1])))
     for s in range(4):
-        bases.step(s)
-    weights.step(0)
-    for s in range(4, 10):
-        bases.step(s)
-    hand_over(near)
+        weights.step(s)
     for cp in x_in:
         cp.wait()
     project([(0, 0)], first=True)
-    project(near)
-    for s in range(10, 14):
-        bases.step(s)
-    hand_over(middle)
-    bases.step(14)
-    weights.step(1)
-    weights.step(2)
-    project(middle)
-    hand_over(last)
-    weights.step(3)
-    project(last)
+    send_levels(NEAR)
+    send_levels(MIDDLE)
+    relay_levels(NEAR)
+    send_levels(FAR)
+    relay_levels(MIDDLE)
+    weights.step(4)
+    hand_over(NEAR)
+    relay_levels(FAR)
+    hand_over(MIDDLE)
+    weights.step(5)
+    project(NEAR[0:2])
+    project(NEAR[2:4])
+    hand_over(FAR)
+    weights.step(6)
+    project(MIDDLE[0:2])
+    project(MIDDLE[2:4])
+    project(MIDDLE[4:6])
+    weights.step(7)
+    project(FAR[0:2])
+    project(FAR[2:4])
+    project(FAR[4:5])
 
     for cp in g_in:
         cp.wait()
@@ -265,16 +313,18 @@
         r, cc = 16 * (j // 2), 512 * (j % 2)
         psend[j] = part[r : r + 16, cc : cc + 512].astype(bf16)
 
-    gq_sum = jnp.zeros((256, 256), f32)
-    go_sum = jnp.zeros((128, 128), f32)
-    for j in range(FS):
-        bqv = ball[j, 0:256, :]
-        bo = jnp.concatenate([ball[j, 256:320, 0:128], ball[j, 256:320, 128:256]], axis=0)
-        gq_sum += dot00(bqv, bqv)
-        go_sum += dot00(bo, bo)
-    gram[0] = gq_sum[0:128, 0:128]
-    gram[1] = gq_sum[128:256, 128:256]
-    gram[2] = go_sum
+    def grams(js, first=False):
+        gq_sum = jnp.zeros((256, 256), f32)
+        go_sum = jnp.zeros((128, 128), f32)
+        for j in js:
+            bqv = ball[j, 0:256, :]
+            bo = outputs_of(j)
+            gq_sum += dot00(bqv, bqv)
+            go_sum += dot00(bo, bo)
+        for i, g in enumerate((gq_sum[0:128, 0:128], gq_sum[128:256, 128:256], go_sum)):
+            gram[i] = g if first else gram[i] + g
+
+    grams(range(0, 4), first=True)
 
     def to_peer(src, dst, send, recv, off):
         return pltpu.make_async_remote_copy(
@@ -291,7 +341,8 @@
         cp = to_peer(psend.at[blk(*off)], precv.at[f], rsend, rrecv, off)
         cp.start()
         scattered.append(cp)
-    weights.step(4)
+    weights.step(8)
+    grams(range(4, FS))
     precv[f] = psend[f]
     for off in OTHERS:
         b = blk(*off)
@@ -300,14 +351,13 @@
     for j in range(1, FS):
         total += precv[j].astype(f32)
     pall[f] = total.astype(bf16)
-    weights.step(5)
     gathered = []
     for off in OTHERS:
         cp = to_peer(pall.at[f], pall.at[f], asend, arecv, off)
         cp.start()
         gathered.append(cp)
-    weights.step(6)
-    weights.step(7)
+    for s in range(9, 13):
+        weights.step(s)
     for cp in m_in:
         cp.wait()
     for off in OTHERS:
@@ -336,8 +386,6 @@
         gd = jnp.dot(gram[i], dd, precision=HIGH, preferred_element_type=f32)
         sums += jnp.sum(dd * gd, keepdims=True)
     sqs[t] = jnp.broadcast_to(sums, (8, 128))
-    weights.step(8)
-    weights.step(9)
 
     def to_tp(src, r):
         return pltpu.make_async_remote_copy(
@@ -354,7 +402,8 @@
         cp = to_tp(sqs.at[t], r)
         cp.start()
         summed.append(cp)
-    weights.step(10)
+    weights.step(13)
+    weights.step(14)
     for r in range(1, TP):
         to_tp(sqs.at[lax.rem(t + r, TP)], TP - r).wait_recv()
     squares = sqs[0]
@@ -363,7 +412,6 @@
     factor = 1.0 / jnp.sqrt(squares[0:1, 0:1] / (3.0 * MODEL * CELL) + floor_mean)
     dn = -factor * d[...]
     dcopy[...] = (learn_rate * dn).astype(bf16)
-    weights.step(11)
     hi = dn.astype(bf16)
     lo = (dn - hi.astype(f32)).astype(bf16)
     bq = ball[f, 0:256, 0:128]
@@ -372,13 +420,10 @@
     stq[...] = dot(bq, hi[:, 0:256]) + dot(bq, lo[:, 0:256])
     stv[...] = dot(bv, hi[:, 256:512]) + dot(bv, lo[:, 256:512])
     sto[...] = dot(bo, hi[:, 512:1024]) + dot(bo, lo[:, 512:1024])
-    for s in range(12, 15):
-        weights.step(s)
     for off in OTHERS:
         weights.block(off)
-    bases.finish()
     weights.finish()
-    for cp in passed + scattered + gathered + summed:
+    for cp in copies + scattered + gathered + summed:
         cp.wait_send()
 
 
@@ -466,7 +511,7 @@
             pltpu.VMEM((128, 1024), f32),
             pltpu.VMEM((TP, 8, 128), f32),
             dma((18,)),
-            dma((60,)), dma((64,)), dma((60,)), dma((64,)), dma((16,)), dma((16,)),
+            dma((60,)), dma((64,)), dma((16,)), dma((16,)), dma((16,)), dma((16,)), dma((64,)), dma((64,)),
             dma((16,)), dma((16,)), dma((16,)), dma((16,)), dma((8,)), dma((8,)),
         ],
         compiler_params=pltpu.CompilerParams(
@@ -493,7 +538,7 @@
                 dma((9,)),
                 dma((48,)),
             ],
-            compiler_params=pltpu.CompilerParams(vmem_limit_bytes=40 * 1024 * 1024),
+            compiler_params=pltpu.CompilerParams(vmem_limit_bytes=12 * 1024 * 1024),
             name="write_copies",
         )(*mid)
     )

time: 72.3 us -> 60.2 us (0.83)
  Pallas kernels: 65.7 us -> 59.4 us
  local copies, waits for them, and re-layouts: 5.42 us -> 0 us
    pallas_call x1, Pallas kernels: 61.8 us -> 55.5 us  [local(): pl.pallas_call(gather_kernel, out_shape=[pltpu.VMEM(s, t) for s, t in mid...]
    unnamed x4 -> x0, local copies, waits for them, and re-layouts: 5.42 us -> none
where the time goes in v3:
time: 60.2 us; the launch traced here: 60.1 us
  Pallas kernels  59.4 us (99%)
  between operations  0.66 us (1%)
    pallas_call x1, Pallas kernels, local(): pl.pallas_call(gather_kernel, out_shape=[pltpu.VMEM(s, t) for s, t in mid...  55.5 us
    pallas_call x1, Pallas kernels, local(): pl.pallas_call(finish_kernel, out_shape=[jax.ShapeDtypeStruct(s, t) for s...  3.88 us

profile of v3, /device:TPU:0, one launch (start us, length us, event | category | flops | bytes accessed | tf_op | source)
XLA Modules:
  0.0 60.1 jit_solution(920333677325723033)
XLA Ops:
  0.7 55.5 %gather_and_reduce.1 = (bf16[16,384,512]{2,1,0:T(8,128)(2,1)S(1)}, bf16[16,320,256]{2,1,0:T(8,128)(2,1)S(1)}, bf16[128,1024]{1,0:T(8,128)(2,1)S(1)}, f32[256,256...) custom-call(bf16[1024,4096]{1,0:T(8,128)(2,1)} %x_h.1, ...), custom_call_target="tpu_custom_call" | custom-call | tf_op jit(solution)/shard_map/gather_and_reduce/pallas_call | solution.py:488
  56.2 3.9 %write_copies.1 = (f32[256,256]{1,0:T(8,128)}, f32[256,256]{1,0:T(8,128)}, f32[128,512]{1,0:T(8,128)}, bf16[4096,256]{1,0:T(8,128)(2,1)}, bf16[4096,256]{1,0:T(8...) custom-call(bf16[16,384,512]{2,1,0:T(8,128)(2,1)S(1)} %get-tuple-ele, ...), custom_call_target="tpu_custom_call" | custom-call | tf_op jit(solution)/shard_map/write_copies/pallas_call | solution.py:529
